TPU v7x, 32 devices: a whole 2x2x4 slice. The times are simulated.
32 devices in a mesh: sp: 8 (over z, y), dp: 4 (over x, core).
Axes of the slice: x: 2, y: 2, z: 4, core: 2. Of those that a mesh axis runs over, the one named last changes fastest.
Arguments:
- queries: bfloat16 [4, 1024, 2048], P('dp', 'sp'), may hold values from -8 to 8
- keys: bfloat16 [4, 1024, 2048], P('dp', 'sp'), may hold values from -8 to 8
- values: bfloat16 [4, 1024, 2048], P('dp', 'sp'), may hold values from -6 to 6
- proj_weight: bfloat16 [2048, 2048], P('sp'), may hold values from -0.125 to 0.125
- residual: bfloat16 [4, 1024, 2048], P('dp', 'sp'), may hold values from -6 to 6
- norm_gain: float32 [2048], replicated, may hold values from 0.1 to 1.9
- route: int32 [4, 1024, 2], P('dp', 'sp'), may hold values from 0 to 7, all different within a row; in each aligned block of 128 rows (0 to 127, 128 to 255, ..., all dimensions but the last counted through in order) at most 64 rows name the same one
- route_weight: float32 [4, 1024, 2], P('dp', 'sp'), may hold values from 0.1 to 1
- w_gate: bfloat16 [8, 2048, 1024], P('sp'), may hold values from -0.125 to 0.125
- w_up: bfloat16 [8, 2048, 1024], P('sp'), may hold values from -0.125 to 0.125
- w_down: bfloat16 [8, 1024, 2048], P('sp'), may hold values from -0.1875 to 0.1875
Outputs:
- mixed: bfloat16 [4, 1024, 2048], P('dp', 'sp')
Inputs may be any that keep to these rules, and one draw needn't show every extreme that they name: `route`: in the rows of one device no expert is named by more than 64 rows, a bound that some block reaches.
All inputs are finite; a program needn't handle non-finite values.
Results may differ from a plain program's by a relative error of at most 0.013.
Values may be sent and summed in bfloat16 or wider, within the bound.
A program may use at most 128 MiB of HBM per device.

v0:
```python
import functools
import math

import jax
import jax.numpy as jnp
from jax import lax
from jax.experimental import pallas as pl
from jax.experimental.pallas import tpu as pltpu
from jax.sharding import PartitionSpec as P

HEADS = 16


EPS = 1e-06

MESH = pl.DeviceIdType.MESH


def attention_kernel(
    n, m, ny, q_ref, k_ref, v_ref, proj_ref, res_ref, gain_ref, stream_ref, normed_ref,
    qbuf, kbuf, vbuf, wbuf, osend, obuf,
    in_send, in_recv, o_send, o_recv, w_send, w_recv,
):
    me, dp = lax.axis_index("sp"), lax.axis_index("dp")
    nz = n // ny
    z, y = me // ny, lax.rem(me, ny)
    cores = 2
    nx = m // cores
    x, core = dp // cores, lax.rem(dp, cores)
    rows, width = q_ref.shape
    cols = width // n
    head = width // HEADS
    heads_here = cols // head
    wcols = wbuf.shape[3]

    def peer(sp, d):
        return {"sp": sp, "dp": d}

    barrier = pltpu.get_barrier_semaphore()
    for off in range(1, n):
        pl.semaphore_signal(barrier, inc=1, device_id=peer(lax.rem(me + off, n), dp), device_id_type=MESH)
    for off in range(1, m):
        pl.semaphore_signal(barrier, inc=1, device_id=peer(me, lax.rem(dp + off, m)), device_id_type=MESH)
    pl.semaphore_wait(barrier, n - 1 + m - 1)

    def my_cols(d):
        return pl.ds(pl.multiple_of(d * cols, cols), cols)

    def row_block(d):
        return pl.ds(pl.multiple_of(d * rows, rows), rows)

    trio = ((k_ref, kbuf), (q_ref, qbuf), (v_ref, vbuf))

    def in_copy(t, off):
        ref, buf = trio[t]
        to = lax.rem(me + off, n)
        return pltpu.make_async_remote_copy(
            src_ref=ref.at[:, my_cols(to)], dst_ref=buf.at[row_block(me), :],
            send_sem=in_send.at[t, off], recv_sem=in_recv.at[t, off],
            device_id=peer(to, dp), device_id_type=MESH,
        )

    def in_wait(t, off):
        ref, buf = trio[t]
        origin = lax.rem(me - off + n, n)
        pltpu.make_async_remote_copy(
            src_ref=ref.at[:, my_cols(me)], dst_ref=buf.at[row_block(origin), :],
            send_sem=in_send.at[t, off], recv_sem=in_recv.at[t, off],
            device_id=peer(origin, dp), device_id_type=MESH,
        ).wait_recv()

    for t in range(3):
        for off in range(1, n):
            in_copy(t, off).start()

    sent = []

    def w_start(cond, q, i, dev, own=False):
        slot = len(sent)
        source = proj_ref.at[:, pl.ds(pl.multiple_of(q * wcols, wcols), wcols)] if own else wbuf.at[q, i]
        copy = pltpu.make_async_remote_copy(
            src_ref=source, dst_ref=wbuf.at[q, i],
            send_sem=w_send.at[slot], recv_sem=w_recv.at[q, i],
            device_id=dev, device_id_type=MESH,
        )
        sent.append((cond, copy))
        if cond is None:
            copy.start()
        else:
            pl.when(cond)(copy.start)

    def w_wait(cond, q, i):
        copy = pltpu.make_async_remote_copy(
            src_ref=wbuf.at[q, i], dst_ref=wbuf.at[q, i],
            send_sem=w_send.at[0], recv_sem=w_recv.at[q, i],
            device_id=peer(me, lax.rem(dp + 1, m)), device_id_type=MESH,
        )
        if cond is None:
            copy.wait_recv()
        else:
            pl.when(cond)(copy.wait_recv)

    up, down = z + 1 < nz, z > 0
    above, below = jnp.minimum(z + 1, nz - 1) * ny + y, jnp.maximum(z - 1, 0) * ny + y
    other = x * cores + lax.rem(core + 1, cores)
    w_start(up, dp, me, peer(above, dp), True)
    w_start(down, dp, me, peer(below, dp), True)
    for o in range(1, ny):
        w_start(None, dp, me, peer(z * ny + lax.rem(y + o, ny), dp), True)

    for q in range(m):
        wbuf[q, me] = proj_ref[:, q * wcols : (q + 1) * wcols]
    for ref, buf in trio:
        buf[row_block(me), :] = ref[:, my_cols(me)]

    def across(cond, i):
        for o in range(1, nx):
            w_start(cond, dp, i, peer(me, lax.rem(x + o, nx) * cores + core), False)
        w_start(cond, dp, i, peer(me, other), False)

    def column(dz, upward):
        def run():
            far = z - dz if upward else z + dz
            cond = far >= 0 if upward else far < nz
            far = jnp.clip(far, 0, nz - 1)
            i = far * ny + y
            w_wait(cond, dp, i)
            more = jnp.logical_and(cond, up if upward else down)
            if dz < nz - 1:
                w_start(more, dp, i, peer(above if upward else below, dp))
            for o in range(1, ny):
                w_start(cond, dp, i, peer(z * ny + lax.rem(y + o, ny), dp))
            across(cond, i)
        return run

    def side(dz, upward, o):
        def run():
            far = z - dz if upward else z + dz
            cond = (far >= 0 if upward else far < nz) if dz else None
            far = jnp.clip(far, 0, nz - 1)
            i = far * ny + lax.rem(y + o, ny)
            w_wait(cond, dp, i)
            across(cond, i)
        return run

    def beyond(off, o):
        def run():
            i = lax.rem(me + off, n)
            q = lax.rem(x + o, nx) * cores + core
            w_wait(None, q, i)
            w_start(None, q, i, peer(me, other))
        return run

    tasks = [side(0, True, o) for o in range(1, ny)]
    for dz in range(1, nz):
        tasks += [column(dz, True), column(dz, False)]
        tasks += [side(dz, way, o) for o in range(1, ny) for way in (True, False)]
    late = [beyond(off, o) for off in range(1, n) for o in range(1, nx)]

    def o_copy(d):
        return pltpu.make_async_remote_copy(
            src_ref=osend.at[d], dst_ref=obuf.at[me],
            send_sem=o_send.at[d], recv_sem=o_recv.at[me],
            device_id=peer(d, dp), device_id_type=MESH,
        )

    for t in range(3):
        for off in range(1, n):
            in_wait(t, off)

    scale = 1.0 / math.sqrt(head)
    row_id = lax.broadcasted_iota(jnp.int32, (rows, rows), 0)
    col_id = lax.broadcasted_iota(jnp.int32, (rows, rows), 1)
    later = (row_id > col_id).astype(jnp.bfloat16)
    inside = col_id < row_id

    def attend(d):
        for h in range(heads_here):
            lanes = slice(h * head, (h + 1) * head)
            query = qbuf[d * rows : (d + 1) * rows, lanes]
            total = jnp.zeros((rows, head), jnp.float32)
            carry = jnp.zeros((rows, 1), jnp.float32)
            for b in range(d, -1, -1):
                block = slice(b * rows, (b + 1) * rows)
                score = lax.dot_general(
                    query, kbuf[block, lanes], (((1,), (1,)), ((), ())),
                    preferred_element_type=jnp.float32,
                ) * scale
                soft = jnp.maximum(score, 0.0) + jnp.log1p(jnp.exp(-jnp.abs(score)))
                log_sigmoid = score - soft
                if b == d:
                    soft = jnp.where(inside, soft, 0.0)
                high = soft.astype(jnp.bfloat16)
                low = (soft - high.astype(jnp.float32)).astype(jnp.bfloat16)
                suffix = jnp.dot(high, later, preferred_element_type=jnp.float32) + jnp.dot(
                    low, later, preferred_element_type=jnp.float32
                )
                weight = jnp.exp(log_sigmoid - suffix - carry)
                if b == d:
                    weight = jnp.where(inside, weight, 0.0)
                carry = carry + suffix[:, 0:1] + soft[:, 0:1]
                total = total + jnp.dot(
                    weight.astype(jnp.bfloat16), vbuf[block, lanes], preferred_element_type=jnp.float32
                )
            osend[d, :, lanes] = total.astype(jnp.bfloat16)

    done = 0
    for d in range(n):
        attend(d)

        @pl.when(me == d)
        def _():
            obuf[me] = osend[d]

        @pl.when(me != d)
        def _():
            o_copy(d).start()

        share = (d + 1) * len(tasks) // n
        for run in tasks[done:share]:
            run()
        done = share
    for run in late:
        run()
    for off in range(1, n):
        i = lax.rem(me + off, n)
        for x_off in range(nx):
            w_wait(None, lax.rem(x + x_off, nx) * cores + lax.rem(core + 1, cores), i)
    for off in range(1, n):
        origin = lax.rem(me - off + n, n)
        pltpu.make_async_remote_copy(
            src_ref=osend.at[0], dst_ref=obuf.at[origin],
            send_sem=o_send.at[0], recv_sem=o_recv.at[origin],
            device_id=peer(origin, dp), device_id_type=MESH,
        ).wait_recv()

    square = jnp.zeros((rows, 1), jnp.float32)
    attended = jnp.concatenate([obuf[i] for i in range(n)], axis=1)
    for q in range(m):
        part = slice(q * wcols, (q + 1) * wcols)
        weights = wbuf[q].reshape(width, wcols)
        acc = jnp.dot(attended, weights, preferred_element_type=jnp.float32)
        stream = (res_ref[:, part].astype(jnp.float32) + acc).astype(jnp.bfloat16)
        stream_ref[:, part] = stream
        stream = stream.astype(jnp.float32)
        square = square + jnp.sum(stream * stream, axis=1, keepdims=True)
    factor = lax.rsqrt(square / width + EPS)
    for q in range(m):
        part = slice(q * wcols, (q + 1) * wcols)
        normed_ref[:, part] = (
            stream_ref[:, part].astype(jnp.float32) * factor * gain_ref[:, part]
        ).astype(jnp.bfloat16)

    for t in range(3):
        for off in range(1, n):
            in_copy(t, off).wait_send()
    for d in range(n):
        @pl.when(me != d)
        def _():
            o_copy(d).wait_send()
    for cond, copy in sent:
        if cond is None:
            copy.wait_send()
        else:
            pl.when(cond)(copy.wait_send)


def attention(queries, keys, values, proj_weight, residual, norm_gain):
    n, m = lax.axis_size("sp"), lax.axis_size("dp")
    rows, width = queries.shape
    cols = width // n
    ny = 1 << ((n.bit_length() - 1) // 2)
    nz, nx = n // ny, m // 2
    copies = 1 + ny + 2 * nz * (ny + nx + 1) + (2 * nz) * ny * nx + n * nx
    bf16 = jnp.bfloat16
    vmem = pl.BlockSpec(memory_space=pltpu.VMEM)
    return pl.pallas_call(
        functools.partial(attention_kernel, n, m, ny),
        out_shape=[jax.ShapeDtypeStruct((rows, width), bf16)] * 2,
        in_specs=[vmem] * 6,
        out_specs=[vmem] * 2,
        scratch_shapes=[
            pltpu.VMEM((n * rows, cols), bf16),
            pltpu.VMEM((n * rows, cols), bf16),
            pltpu.VMEM((n * rows, cols), bf16),
            pltpu.VMEM((m, n, cols, width // m), bf16),
            pltpu.VMEM((n, rows, cols), bf16),
            pltpu.VMEM((n, rows, cols), bf16),
            pltpu.SemaphoreType.DMA((3, n)),
            pltpu.SemaphoreType.DMA((3, n)),
            pltpu.SemaphoreType.DMA((n,)),
            pltpu.SemaphoreType.DMA((n,)),
            pltpu.SemaphoreType.DMA((copies,)),
            pltpu.SemaphoreType.DMA((m, n)),
        ],
        compiler_params=pltpu.CompilerParams(
            collective_id=0, has_side_effects=True, vmem_limit_bytes=50 * 1024 * 1024
        ),
    )(queries, keys, values, proj_weight, residual, norm_gain.reshape(1, width))


def body(
    queries,
    keys,
    values,
    proj_weight,
    residual,
    norm_gain,
    route,
    route_weight,
    w_gate,
    w_up,
    w_down,
):
    seq_span = lax.axis_size("sp")
    rows = queries.shape[1]
    width = queries.shape[2]
    stream, normed = attention(
        queries[0], keys[0], values[0], proj_weight, residual[0], norm_gain
    )
    stream_f = stream.astype(jnp.float32)
    capacity = 4 * rows // seq_span
    chosen = route[0].reshape(rows * 2)
    one_hot = (chosen[:, None] == jnp.arange(seq_span, dtype=jnp.int32)[None, :]).astype(jnp.int32)
    earlier = jnp.cumsum(one_hot, axis=0) - one_hot
    slot = jnp.sum(earlier * one_hot, axis=1)
    target = chosen * capacity + slot
    source_row = jnp.arange(rows * 2, dtype=jnp.int32) // 2
    slot_source = jnp.zeros((seq_span * capacity,), jnp.int32).at[target].set(source_row)
    slot_used = jnp.zeros((seq_span * capacity,), jnp.bool_).at[target].set(True)
    outgoing = jnp.where(slot_used[:, None], normed[slot_source], jnp.zeros((), jnp.bfloat16))
    outgoing = outgoing.reshape(seq_span, capacity, width)
    arrived = lax.all_to_all(outgoing, "sp", split_axis=0, concat_axis=0, tiled=True)
    senders, slots, features = arrived.shape
    flat = arrived.reshape(senders * slots, features)
    gate = jnp.dot(flat, w_gate[0], preferred_element_type=jnp.float32)
    upper = jnp.dot(flat, w_up[0], preferred_element_type=jnp.float32)
    hidden = (jax.nn.silu(gate) * upper).astype(jnp.bfloat16)
    result = jnp.dot(hidden, w_down[0], preferred_element_type=jnp.float32).astype(jnp.bfloat16)
    returned = lax.all_to_all(
        result.reshape(senders, slots, features), "sp", split_axis=0, concat_axis=0, tiled=True
    )
    picked = returned.reshape(seq_span * capacity, width)[target].reshape(rows, 2, width)
    mixed = stream_f + jnp.sum(route_weight[0][:, :, None] * picked.astype(jnp.float32), axis=1)
    return mixed.astype(jnp.bfloat16)[None]


def solution(mesh):
    return jax.shard_map(
        body,
        mesh=mesh,
        in_specs=(
            P("dp", "sp", None),
            P("dp", "sp", None),
            P("dp", "sp", None),
            P("sp", None),
            P("dp", "sp", None),
            P(),
            P("dp", "sp", None),
            P("dp", "sp", None),
            P("sp", None, None),
            P("sp", None, None),
            P("sp", None, None),
        ),
        out_specs=P("dp", "sp", None),
        check_vma=False,
    )
```

profile of v0, /device:TPU:0, one launch (start us, length us, event | category | flops | bytes accessed | tf_op | source)
XLA Modules:
  0.0 232.7 jit_solution(4342108567677446756)
XLA Ops:
  0.0 0.8 copy.15
  0.8 0.1 eq.29
  0.9 0.1 eq.25
  1.1 0.7 broadcast_multiply_fusion
  1.8 0.6 reduce-window.6
  2.3 0.2 slice_reduce_fusion
  2.6 0.1 copy.14
  2.7 0.1 mul.40
  2.9 0.1 fusion.15
  3.0 1.4 scatter_custom_fusion.1
  4.4 1.5 scatter_custom_fusion
  5.9 0.1 broadcast_in_dim.33
  6.0 0.0 copy-start
  6.0 1.0 copy-done
  7.0 0.0 copy-start.1
  7.0 1.0 copy-done.1
  8.1 0.0 copy-start.2
  8.1 1.0 copy-done.2
  9.1 0.0 copy-start.3
  9.1 1.0 copy-done.3
  10.1 0.0 copy-start.4
  10.2 0.7 copy-done.4
  10.8 89.1 %shard_map.109 = (bf16[128,2048]{1,0:T(8,128)(2,1)S(1)}, bf16[128,2048]{1,0:T(8,128)(2,1)S(1)}) custom-call(bf16[128,2048]{1,0:T(8,128)(2,1)S(1)} %bitcast.39, bf16[128,2048]{1,0:T(8,128)(2,1)S(1)} %bitcast.40, bf16[128,2048]{1,0:T(8,128)(2,1)S(1)} %bitcast.41, bf16[256,2048]{1,0:T(8,128)(2,1)} %proj_ref.1, bf16[128,2048]{1,0:T(8,128)(2,1)S(1)} %bitcast.42, ...), custom_call_target="tpu_custom_call" | custom-call | tf_op jit(solution)/shard_map/pallas_call | solution.py:277
  100.0 2.5 %gather_fusion = bf16[512,2048]{1,0:T(8,128)(2,1)S(1)} fusion(bf16[128,2048]{1,0:T(8,128)(2,1)S(1)} %get-tuple-element.8, s32[1024]{0:T(1024)S(1)} %pad_clamp_fusion.1), kind=kCustom, calls=%fused_computation | custom fusion | bytes 4196352 | tf_op jit(solution)/shard_map/gather | solution.py:331
  102.5 0.2 broadcast_select_fusion
  102.7 0.0 copy-start.6
  102.7 54.6 %all_to_all.10 = bf16[8,64,2048]{2,1,0:T(8,128)(2,1)S(1)} all-to-all(bf16[8,64,2048]{2,1,0:T(8,128)(2,1)S(1)} %broadcast_select_fusion), channel_id=1, replica_groups=mesh['sp'=8,'dp'=4] {'sp'}, dimensions={0} | all-to-all | bytes 4194304 | tf_op jit(solution)/shard_map/all_to_all | solution.py:333
  157.3 0.0 copy-done.6
  157.3 3.7 %fusion.4 = f32[512,1024]{1,0:T(8,128)} fusion(bf16[512,2048]{1,0:T(8,128)(2,1)S(1)} %bitcast.47, bf16[1,2048,1024]{2,1,0:T(8,128)(2,1)S(1)} %copy-done.6), kind=kOutput, calls=%fused_computation.8 | convolution fusion | flops 2147483648 | bytes 8388608 | tf_op jit(solution)/shard_map/dot_general | solution.py:336
  161.0 9.9 %fusion.6 = bf16[512,2048]{1,0:T(8,128)(2,1)} fusion(bf16[1,1024,2048]{2,1,0:T(8,128)(2,1)} %param.21, f32[512,1024]{1,0:T(8,128)} %fusion.4, bf16[512,2048]{1,0:T(8,128)(2,1)S(1)} %bitcast.48, bf16[1,2048,1024]{2,1,0:T(8,128)(2,1)} %param.20), kind=kOutput, calls=%fused_computation.10 | convolution fusion | flops 4299161600 | bytes 14680064 | tf_op jit(solution)/shard_map/dot_general | solution.py:339
  170.9 0.0 copy-start.5
  170.9 4.4 %all-to-all-start.1 = ((bf16[8,64,2048]{2,1,0:T(8,128)(2,1)}), bf16[8,64,2048]{2,1,0:T(8,128)(2,1)S(1)}, u32[]{:S(2)}, u32[]{:S(2)}) async-start(bf16[8,64,2048]{2,1,0:T(8,128)(2,1)} %bitcast.46), calls=%async_computation.1 | async-start | bytes 4194304 | tf_op jit(solution)/shard_map/all_to_all | solution.py:340
  175.3 0.0 copy-done.5
  175.3 0.1 copy.13
  175.4 48.4 %all-to-all-done.1 = bf16[8,64,2048]{2,1,0:T(8,128)(2,1)S(1)} async-done(((bf16[8,64,2048]{2,1,0:T(8,128)(2,1)}), bf16[8,64,2048]{2,1,0:T(8,128)(2,1)S(1)}, u32[]{:S(2)}, u32[]{:S(2)}) %all-to-all-start.1) | async-done | bytes 2097184 | tf_op jit(solution)/shard_map/all_to_all | solution.py:340
  223.8 2.3 %gather_fusion.1 = bf16[256,2048]{1,0:T(8,128)(2,1)} fusion(bf16[512,2048]{1,0:T(8,128)(2,1)S(1)} %bitcast.44, s32[1024]{0:T(1024)S(1)} %pad_clamp_fusion), kind=kCustom, calls=%fused_computation.1 | custom fusion | bytes 2098176 | tf_op jit(solution)/shard_map/gather | solution.py:343
  226.2 2.4 %reshape.74 = f32[128,2,2048]{2,1,0:T(2,128)S(1)} reshape(bf16[256,2048]{1,0:T(8,128)(2,1)} %gather_fusion.1) | data formatting | bytes 3145728 | tf_op jit(solution)/shard_map/convert_element_type | solution.py:344
  228.5 3.2 %multiply_reduce_fusion = f32[128,2048]{1,0:T(8,128)S(1)} fusion(f32[128,2,2048]{2,1,0:T(2,128)S(1)} %reshape.74, f32[128,2]{1,0:T(8,128)S(1)} %copy.13), kind=kLoop, calls=%fused_computation.11 | loop fusion | flops 786432 | bytes 3146752 | tf_op jit(solution)/shard_map/reduce_sum | solution.py:344
  231.7 0.9 fusion.13
  (9 shorter events, 0.1 us)
Async XLA Ops:
  6.0 1.0 copy-start
  7.0 1.0 copy-start.1
  8.1 1.0 copy-start.2
  9.1 1.0 copy-start.3
  10.1 0.7 copy-start.4
  102.7 54.6 %copy-start.6 = (bf16[1,2048,1024]{2,1,0:T(8,128)(2,1)S(1)}, bf16[1,2048,1024]{2,1,0:T(8,128)(2,1)}, u32[]{:S(2)}) copy-start(bf16[1,2048,1024]{2,1,0:T(8,128)(2,1)} %param.19) | copy-start | bytes 12582916
  170.9 4.4 %copy-start.5 = (f32[1,128,2]{1,2,0:T(2,128)S(1)}, f32[1,128,2]{1,2,0:T(2,128)}, u32[]{:S(2)}) copy-start(f32[1,128,2]{1,2,0:T(2,128)} %param.18) | copy-start | bytes 3076
  170.9 52.9 %all-to-all-start.1 = ((bf16[8,64,2048]{2,1,0:T(8,128)(2,1)}), bf16[8,64,2048]{2,1,0:T(8,128)(2,1)S(1)}, u32[]{:S(2)}, u32[]{:S(2)}) async-start(bf16[8,64,2048]{2,1,0:T(8,128)(2,1)} %bitcast.46), calls=%async_computation.1 | async-start | bytes 4194304 | tf_op jit(solution)/shard_map/all_to_all | solution.py:340
where the time goes:
time: 233 us
  Pallas kernels  89.1 us (38%)
  blocking collectives  54.6 us (23%)
  waiting for transfers between devices  48.4 us (21%)
  local copies, waits for them, and re-layouts  16.7 us (7%)
  matrix products  13.6 us (6%)
  other arithmetic  5.73 us (2%)
  starting transfers between devices  4.42 us (2%)
    pallas_call x1, Pallas kernels, attention(): pl.pallas_call(functools.partial(attention_kernel, n, m, ny), out_shape=[...  89.1 us
    all_to_all x1, blocking collectives, body(): lax.all_to_all(outgoing, 'sp', split_axis=0, concat_axis=0, tiled=True)  54.6 us
    all_to_all x1, waiting for transfers between devices, body(): lax.all_to_all(result.reshape(senders, slots, features), 'sp', split_axis...  48.4 us
    dot_general x1, matrix products, body(): jnp.dot(hidden, w_down[0], preferred_element_type=jnp.float32)  9.89 us
    unnamed x15, local copies, waits for them, and re-layouts  5.66 us
  transfers between devices with their start and end apart: 1, of which 1 were waited for; matrix products, arithmetic and copies ran while one was open for 0% of the time, Pallas kernels for 0%

commit v1 on v0

--- a/solution.py
+++ b/solution.py
@@ -299,6 +299,181 @@
     )(queries, keys, values, proj_weight, residual, norm_gain.reshape(1, width))
 
 
+def flipped(number, off, n):
+    result = number
+    bit = 1
+    while bit < n:
+        result = result + bit * lax.rem(off // bit, 2) * (1 - 2 * lax.rem(number // bit, 2))
+        bit *= 2
+    return result
+
+
+def expert_kernel(
+    n, normed_ref, stream_ref, target_ref, flat_ref, share_ref, gate_hbm, up_hbm, down_hbm, out_ref,
+    gate_ref, up_ref, down_ref, outgoing, inbox, outbox, back, total,
+    load_sem, there_send, there_recv, back_send, back_recv,
+):
+    me, dp = lax.axis_index("sp"), lax.axis_index("dp")
+    rows, width = normed_ref.shape
+    capacity = inbox.shape[1]
+    pairs = n // 2
+
+    loads = [
+        pltpu.make_async_copy(gate_hbm.at[0], gate_ref, load_sem.at[0]),
+        pltpu.make_async_copy(up_hbm.at[0], up_ref, load_sem.at[1]),
+        pltpu.make_async_copy(down_hbm.at[0], down_ref, load_sem.at[2]),
+    ]
+    for load in loads:
+        load.start()
+
+    barrier = pltpu.get_barrier_semaphore()
+    for off in range(1, n):
+        pl.semaphore_signal(
+            barrier, inc=1, device_id={"sp": lax.rem(me + off, n), "dp": dp}, device_id_type=MESH
+        )
+
+    def gathered(expert):
+        slot = lax.broadcasted_iota(jnp.int32, (capacity, rows), 0) + expert * capacity
+        chosen = jnp.logical_or(flat_ref[0:1, :] == slot, flat_ref[1:2, :] == slot)
+        return jnp.dot(
+            chosen.astype(jnp.bfloat16), normed_ref[...], preferred_element_type=jnp.float32
+        ).astype(jnp.bfloat16)
+
+    def there(off):
+        return pltpu.make_async_remote_copy(
+            src_ref=outgoing.at[off], dst_ref=inbox.at[off],
+            send_sem=there_send.at[off], recv_sem=there_recv.at[off],
+            device_id={"sp": flipped(me, off, n), "dp": dp}, device_id_type=MESH,
+        )
+
+    def home(off):
+        return pltpu.make_async_remote_copy(
+            src_ref=outbox.at[off], dst_ref=back.at[off],
+            send_sem=back_send.at[off], recv_sem=back_recv.at[off],
+            device_id={"sp": flipped(me, off, n), "dp": dp}, device_id_type=MESH,
+        )
+
+    pl.semaphore_wait(barrier, n - 1)
+
+    @pl.loop(0, n)
+    def _(step):
+        pair = lax.rem(pairs - step // 2, pairs)
+        off = pair * 2 + 1 - lax.rem(step, 2)
+        block = gathered(flipped(me, off, n))
+
+        @pl.when(off > 0)
+        def _():
+            outgoing[off] = block
+            there(off).start()
+
+        @pl.when(off == 0)
+        def _():
+            inbox[0] = block
+
+    for load in loads:
+        load.wait()
+
+    hidden_width = gate_ref.shape[1]
+    piece = min(512, hidden_width)
+
+    @pl.loop(0, pairs)
+    def _(step):
+        pair = lax.rem(pairs - step, pairs)
+
+        @pl.when(pair > 0)
+        def _():
+            there(pair * 2).wait_recv()
+
+        there(pair * 2 + 1).wait_recv()
+        arrived = inbox[pl.ds(pair * 2, 2)].reshape(2 * capacity, width)
+        hidden = []
+        for first in range(0, hidden_width, piece):
+            part = slice(first, first + piece)
+            gate = jnp.dot(arrived, gate_ref[:, part], preferred_element_type=jnp.float32)
+            upper = jnp.dot(arrived, up_ref[:, part], preferred_element_type=jnp.float32)
+            hidden.append((jax.nn.silu(gate) * upper).astype(jnp.bfloat16))
+        hidden = jnp.concatenate(hidden, axis=1)
+        for first in range(0, width, piece):
+            part = slice(first, first + piece)
+            result = jnp.dot(hidden, down_ref[:, part], preferred_element_type=jnp.float32)
+            outbox[pl.ds(pair * 2, 2), :, part] = result.astype(jnp.bfloat16).reshape(
+                2, capacity, piece
+            )
+
+        @pl.when(pair > 0)
+        def _():
+            home(pair * 2).start()
+
+        @pl.when(pair == 0)
+        def _():
+            back[0] = outbox[0]
+
+        home(pair * 2 + 1).start()
+
+    total[...] = stream_ref[...].astype(jnp.float32)
+
+    @pl.loop(0, pairs)
+    def _(step):
+        pair = lax.rem(pairs - step, pairs)
+
+        @pl.when(pair > 0)
+        def _():
+            home(pair * 2).wait_recv()
+
+        home(pair * 2 + 1).wait_recv()
+        slot = lax.broadcasted_iota(jnp.int32, (rows, 2 * capacity), 1)
+        even, odd = flipped(me, pair * 2, n), flipped(me, pair * 2 + 1, n)
+        slot = jnp.where(slot < capacity, slot + even * capacity, slot - capacity + odd * capacity)
+        first = (target_ref[:, 0:1] == slot).astype(jnp.bfloat16)
+        second = (target_ref[:, 1:2] == slot).astype(jnp.bfloat16)
+        for start in range(0, width, piece):
+            part = slice(start, start + piece)
+            block = back[pl.ds(pair * 2, 2), :, part].reshape(2 * capacity, piece)
+            total[:, part] += share_ref[:, 0:1] * jnp.dot(
+                first, block, preferred_element_type=jnp.float32
+            ) + share_ref[:, 1:2] * jnp.dot(second, block, preferred_element_type=jnp.float32)
+
+    out_ref[...] = total[...].astype(jnp.bfloat16)
+
+    @pl.loop(1, n)
+    def _(off):
+        there(off).wait_send()
+        home(off).wait_send()
+
+
+def experts(normed, stream, target, share, w_gate, w_up, w_down):
+    n = lax.axis_size("sp")
+    rows, width = normed.shape
+    capacity = 4 * rows // n
+    hidden = w_gate.shape[2]
+    bf16 = jnp.bfloat16
+    vmem = pl.BlockSpec(memory_space=pltpu.VMEM)
+    return pl.pallas_call(
+        functools.partial(expert_kernel, n),
+        out_shape=jax.ShapeDtypeStruct((rows, width), bf16),
+        in_specs=[vmem] * 5 + [pl.BlockSpec(memory_space=pl.ANY)] * 3,
+        out_specs=vmem,
+        scratch_shapes=[
+            pltpu.VMEM((width, hidden), bf16),
+            pltpu.VMEM((width, hidden), bf16),
+            pltpu.VMEM((hidden, width), bf16),
+            pltpu.VMEM((n, capacity, width), bf16),
+            pltpu.VMEM((n, capacity, width), bf16),
+            pltpu.VMEM((n, capacity, width), bf16),
+            pltpu.VMEM((n, capacity, width), bf16),
+            pltpu.VMEM((rows, width), jnp.float32),
+            pltpu.SemaphoreType.DMA((3,)),
+            pltpu.SemaphoreType.DMA((n,)),
+            pltpu.SemaphoreType.DMA((n,)),
+            pltpu.SemaphoreType.DMA((n,)),
+            pltpu.SemaphoreType.DMA((n,)),
+        ],
+        compiler_params=pltpu.CompilerParams(
+            collective_id=1, has_side_effects=True, vmem_limit_bytes=50 * 1024 * 1024
+        ),
+    )(normed, stream, target, target.T, share, w_gate, w_up, w_down)
+
+
 def body(
     queries,
     keys,
@@ -318,31 +493,13 @@
     stream, normed = attention(
         queries[0], keys[0], values[0], proj_weight, residual[0], norm_gain
     )
-    stream_f = stream.astype(jnp.float32)
     capacity = 4 * rows // seq_span
     chosen = route[0].reshape(rows * 2)
     one_hot = (chosen[:, None] == jnp.arange(seq_span, dtype=jnp.int32)[None, :]).astype(jnp.int32)
     earlier = jnp.cumsum(one_hot, axis=0) - one_hot
     slot = jnp.sum(earlier * one_hot, axis=1)
-    target = chosen * capacity + slot
-    source_row = jnp.arange(rows * 2, dtype=jnp.int32) // 2
-    slot_source = jnp.zeros((seq_span * capacity,), jnp.int32).at[target].set(source_row)
-    slot_used = jnp.zeros((seq_span * capacity,), jnp.bool_).at[target].set(True)
-    outgoing = jnp.where(slot_used[:, None], normed[slot_source], jnp.zeros((), jnp.bfloat16))
-    outgoing = outgoing.reshape(seq_span, capacity, width)
-    arrived = lax.all_to_all(outgoing, "sp", split_axis=0, concat_axis=0, tiled=True)
-    senders, slots, features = arrived.shape
-    flat = arrived.reshape(senders * slots, features)
-    gate = jnp.dot(flat, w_gate[0], preferred_element_type=jnp.float32)
-    upper = jnp.dot(flat, w_up[0], preferred_element_type=jnp.float32)
-    hidden = (jax.nn.silu(gate) * upper).astype(jnp.bfloat16)
-    result = jnp.dot(hidden, w_down[0], preferred_element_type=jnp.float32).astype(jnp.bfloat16)
-    returned = lax.all_to_all(
-        result.reshape(senders, slots, features), "sp", split_axis=0, concat_axis=0, tiled=True
-    )
-    picked = returned.reshape(seq_span * capacity, width)[target].reshape(rows, 2, width)
-    mixed = stream_f + jnp.sum(route_weight[0][:, :, None] * picked.astype(jnp.float32), axis=1)
-    return mixed.astype(jnp.bfloat16)[None]
+    target = (chosen * capacity + slot).reshape(rows, 2)
+    return experts(normed, stream, target, route_weight[0], w_gate, w_up, w_down)[None]
 
 
 def solution(mesh):

time: 233 us -> 200 us (0.86)
  Pallas kernels: 89.1 us -> 190 us
  blocking collectives: 54.6 us -> 0 us
  waiting for transfers between devices: 48.4 us -> 0 us
  matrix products: 13.6 us -> 0 us
  local copies, waits for them, and re-layouts: 16.7 us -> 8.03 us
  starting transfers between devices: 4.42 us -> 0 us
  other arithmetic: 5.73 us -> 1.42 us
    pallas_call x0 -> x1, Pallas kernels: none -> 101 us  [experts(): pl.pallas_call(functools.partial(expert_kernel, n), out_shape=jax.ShapeDt...]
    all_to_all x1 -> x0, blocking collectives: 54.6 us -> none  [body(): lax.all_to_all(outgoing, 'sp', split_axis=0, concat_axis=0, tiled=True)]
    all_to_all x1 -> x0, waiting for transfers between devices: 48.4 us -> none  [body(): lax.all_to_all(result.reshape(senders, slots, features), 'sp', split_axis...]
    dot_general x2 -> x0, matrix products: 13.6 us -> none  [the longest x1 9.89 us: body(): jnp.dot(hidden, w_down[0], preferred_element_type=jnp.float32)]
    gather x2 -> x0, local copies, waits for them, and re-layouts: 4.81 us -> none  [the longest x1 2.47 us: body(): normed[slot_source]]
    all_to_all x1 -> x0, starting transfers between devices: 4.42 us -> none  [body(): lax.all_to_all(result.reshape(senders, slots, features), 'sp', split_axis...]
    reduce_sum x1 -> x0, other arithmetic: 3.16 us -> none  [body(): jnp.sum(route_weight[0][:, :, None] * picked.astype(jnp.float32), axis=1)]
    scatter x2 -> x0, local copies, waits for them, and re-layouts: 2.88 us -> none  [the longest x1 1.49 us: body(): jnp.zeros((seq_span * capacity,), jnp.bool_).at[target].set(True)]
  transfers between devices with their start and end apart: 1 -> 0, of which waited for: 1 -> 0; matrix products, arithmetic and copies ran while one was open for 0% -> 0% of each run, Pallas kernels for 0% -> 0%
where the time goes in v1:
time: 200 us
  Pallas kernels  190 us (95%)
  local copies, waits for them, and re-layouts  8.03 us (4%)
    pallas_call x1, Pallas kernels, experts(): pl.pallas_call(functools.partial(expert_kernel, n), out_shape=jax.ShapeDt...  101 us
    pallas_call x1, Pallas kernels, attention(): pl.pallas_call(functools.partial(attention_kernel, n, m, ny), out_shape=[...  89.2 us
    unnamed x13, local copies, waits for them, and re-layouts  7.22 us

profile of v1, /device:TPU:0, one launch (start us, length us, event | category | flops | bytes accessed | tf_op | source)
XLA Modules:
  0.0 199.5 jit_solution(1986319435659235268)
XLA Ops:
  0.0 0.8 copy.14
  0.8 0.1 eq.29
  0.9 0.1 eq.25
  1.1 0.6 reduce-window.6
  1.7 0.2 slice_reduce_fusion
  1.9 0.1 fusion.1
  2.0 0.1 reduce_sum.12
  2.2 0.1 copy.16
  2.2 0.7 bitcast_add_fusion
  2.9 0.1 copy.18.target_ref
  3.0 0.8 copy.17
  3.8 0.0 copy-start
  3.8 1.0 copy-done
  4.9 0.0 copy-start.1
  4.9 1.0 copy-done.1
  5.9 0.0 copy-start.2
  5.9 1.0 copy-done.2
  7.0 0.0 copy-start.3
  7.0 1.0 copy-done.3
  8.0 0.0 copy-start.4
  8.0 0.7 copy-done.4
  8.7 89.2 %shard_map.109 = (bf16[128,2048]{1,0:T(8,128)(2,1)S(1)}, bf16[128,2048]{1,0:T(8,128)(2,1)S(1)}) custom-call(bf16[128,2048]{1,0:T(8,128)(2,1)S(1)} %bitcast.19, bf16[128,2048]{1,0:T(8,128)(2,1)S(1)} %bitcast.20, bf16[128,2048]{1,0:T(8,128)(2,1)S(1)} %bitcast.21, bf16[256,2048]{1,0:T(8,128)(2,1)} %proj_ref.1, bf16[128,2048]{1,0:T(8,128)(2,1)S(1)} %bitcast.22, ...), custom_call_target="tpu_custom_call" | custom-call | tf_op jit(solution)/shard_map/pallas_call | solution.py:277
  97.9 100.9 %shard_map.110 = bf16[128,2048]{1,0:T(8,128)(2,1)S(1)} custom-call(bf16[128,2048]{1,0:T(8,128)(2,1)S(1)} %get-tuple-element.7.normed_ref, bf16[128,2048]{1,0:T(8,128)(2,1)S(1)} %get-tuple-element.8.stream_ref, s32[128,2]{1,0:T(8,128)S(1)} %copy.18.target_ref, s32[2,128]{1,0:T(2,128)S(1)} %bitcast.24, f32[128,2]{1,0:T(8,128)S(1)} %bitcast.23, ...), custom_call_target="tpu_custom_call" | custom-call | tf_op jit(solution)/shard_map/pallas_call | solution.py:451
  198.7 0.8 copy.20
  (3 shorter events, 0.0 us)
Async XLA Ops:
  3.8 1.0 copy-start
  4.9 1.0 copy-start.1
  5.9 1.0 copy-start.2
  7.0 1.0 copy-start.3
  8.0 0.7 copy-start.4
